TPU v7x, 32 devices: a whole 2x2x4 slice. The times are simulated.
32 devices in a mesh: sp: 8 (over z, y), tp: 4 (over x, core).
Axes of the slice: x: 2, y: 2, z: 4, core: 2. Of those that a mesh axis runs over, the one named last changes fastest.
Arguments:
- tokens: bfloat16 [4096, 2048], P(('sp', 'tp')), may hold values from -6 to 6
- norm_gain: bfloat16 [2048], replicated, may hold values from 0.099609375 to 1.8984375
- proj_x: bfloat16 [2048, 2048], P('sp', 'tp'), may hold values from -0.125 to 0.125
- gate_projection: bfloat16 [2048, 2048], P('sp', 'tp'), may hold values from -0.125 to 0.125
- conv_taps: bfloat16 [4, 2048], P(None, 'tp'), may hold values from -3 to 3
- gate_recur: bfloat16 [8, 256, 256], P('tp'), may hold values from -0.375 to 0.375
- gate_input: bfloat16 [8, 256, 256], P('tp'), may hold values from -0.375 to 0.375
- decay_param: float32 [2048], P('tp'), may hold values from 4 to 25
- decay_shift: float32 [8, 4096], P('tp', 'sp'), may hold values from -1.3 to 0, as said below
- proj_out: bfloat16 [2048, 2048], P('tp', 'sp'), may hold values from -0.125 to 0.125
Outputs:
- mixed_out: bfloat16 [4096, 2048], P(('sp', 'tp'))
Inputs may be any that keep to these rules, and one draw needn't show every extreme that they name: `decay_shift`: added log-decays, never positive.
All inputs are finite; a program needn't handle non-finite values.
Results may differ from a plain program's by a relative error of at most 0.015.
Values may be sent and summed in bfloat16 or wider, within the bound.
A program may use at most 128 MiB of HBM per device.

v0:
```python
import jax
import jax.numpy as jnp
from jax import lax
from jax.sharding import PartitionSpec as P

HEAD = 256
CONV = 4


def shifted(block, axis, distance):
    devices = range(lax.axis_size(axis))
    route = [(i - distance, i) for i in devices if i - distance in devices]
    return lax.ppermute(block, axis, route)


def carried_in(array, axis, combine, identity):
    size, index = (lax.axis_size(axis), lax.axis_index(axis))
    everything = jax.tree.map(lambda part: lax.all_gather(part, axis), array)
    start = jax.tree.map(
        lambda part, zero: jnp.broadcast_to(jnp.asarray(zero, part.dtype), part.shape),
        array,
        identity,
    )

    def turn(k, before):
        reached = k < index
        new = combine(before, jax.tree.map(lambda part: part[k], everything))
        return jax.tree.map(lambda a, b: jnp.where(reached, a, b), new, before)

    return lax.fori_loop(0, size, turn, start)


def rms_norm(values, norm_gain):
    floats = values.astype(jnp.float32)
    scaled = floats * lax.rsqrt(jnp.mean(floats * floats, axis=-1, keepdims=True) + 1e-06)
    return (scaled * norm_gain.astype(jnp.float32)).astype(jnp.bfloat16)


def combine_pair(earlier, later):
    return (earlier[0] * later[0], later[0] * earlier[1] + later[1])


def on_device(
    tokens,
    norm_gain,
    proj_x,
    gate_projection,
    conv_taps,
    gate_recur,
    gate_input,
    decay_param,
    decay_shift,
    proj_out,
):
    normed = rms_norm(tokens, norm_gain)
    full_x, full_gate = (
        lax.all_gather(proj_x, "sp", axis=0, tiled=True),
        lax.all_gather(gate_projection, "sp", axis=0, tiled=True),
    )
    local_width = proj_x.shape[1]
    piece = lax.all_gather(normed, "tp", axis=0, tiled=True)
    branch_piece = jnp.dot(piece, full_x, preferred_element_type=jnp.float32).astype(jnp.bfloat16)
    gating_piece = jnp.dot(piece, full_gate, preferred_element_type=jnp.float32).astype(
        jnp.bfloat16
    )
    joined = jnp.concatenate([branch_piece, gating_piece], axis=1)
    branch = joined[:, :local_width]
    gating = joined[:, local_width:]
    row_count = branch.shape[0]
    tail_rows = shifted(branch[row_count - CONV + 1 :], "sp", 1)
    extended = jnp.concatenate([tail_rows, branch], axis=0)
    conv_sum = jnp.zeros((row_count, local_width), jnp.float32)
    for tap_index in range(CONV):
        conv_sum = conv_sum + extended[tap_index : tap_index + row_count].astype(
            jnp.float32
        ) * conv_taps[tap_index].astype(jnp.float32)
    conved = conv_sum.astype(jnp.bfloat16)
    head_count = gate_recur.shape[0]
    grouped = conved.reshape(row_count, head_count, HEAD)
    recur = jax.nn.sigmoid(
        jnp.einsum("thi,hij->thj", grouped, gate_recur, preferred_element_type=jnp.float32)
    )
    inlet = jax.nn.sigmoid(
        jnp.einsum("thi,hij->thj", grouped, gate_input, preferred_element_type=jnp.float32)
    )
    decay_rate = jax.nn.softplus(-decay_param).reshape(head_count, HEAD)
    log_decay = (-8.0 * recur * decay_rate[None] + jnp.transpose(decay_shift)[:, :, None]).reshape(
        row_count, local_width
    )
    decay = jnp.exp(log_decay)
    drive = (
        jnp.sqrt(-jnp.expm1(2.0 * log_decay))
        * inlet.reshape(row_count, local_width)
        * conved.astype(jnp.float32)
    )
    identity = (jnp.ones((local_width,), jnp.float32), jnp.zeros((local_width,), jnp.float32))
    cumulative, local_state = lax.associative_scan(combine_pair, (decay, drive), axis=0)
    carried = carried_in(
        (cumulative[row_count - 1], local_state[row_count - 1]), "sp", combine_pair, identity
    )
    states = local_state + cumulative * carried[1][None, :]
    mixed = (states * jax.nn.gelu(gating.astype(jnp.float32))).astype(jnp.bfloat16)
    out_cols = lax.all_gather(proj_out, "sp", axis=1, tiled=True)
    return lax.psum_scatter(
        jnp.dot(mixed, out_cols, preferred_element_type=jnp.float32).astype(jnp.bfloat16),
        "tp",
        scatter_dimension=0,
        tiled=True,
    )


def solution(mesh):
    in_specs = (
        P(("sp", "tp"), None),
        P(),
        P("sp", "tp"),
        P("sp", "tp"),
        P(None, "tp"),
        P("tp", None, None),
        P("tp", None, None),
        P("tp"),
        P("tp", "sp"),
        P("tp", "sp"),
    )
    out_specs = P(("sp", "tp"), None)
    return jax.shard_map(
        on_device, mesh=mesh, in_specs=in_specs, out_specs=out_specs, check_vma=False
    )
```

profile of v0, /device:TPU:0, one launch (start us, length us, event | category | flops | bytes accessed | tf_op | source)
XLA Modules:
  0.0 287.4 jit_solution(4033228351637639462)
XLA Ops:
  6.5 1.3 fusion.11
  8.5 2.0 fusion.13
  12.7 23.3 %all-gather.7.cloned.1.call-done = bf16[512,2048]{1,0:T(8,128)(2,1)} async-done(((bf16[128,2048]{1,0:T(8,128)(2,1)}), bf16[512,2048]{1,0:T(8,128)(2,1)}) %all-gather.7.cloned.1.call-update) | async-done | bytes 2097168 | tf_op jit(solution)/shard_map/all_gather | solution.py:61
  36.0 51.2 %all-gather.9.cloned.1.call-done = bf16[2048,512]{1,0:T(8,128)(2,1)} async-done(((bf16[256,512]{1,0:T(8,128)(2,1)}), bf16[2048,512]{1,0:T(8,128)(2,1)}) %all-gather.9.cloned.1.call-update) | async-done | bytes 2097168 | tf_op jit(solution)/shard_map/all_gather | solution.py:57
  87.3 3.5 %convolution_convert_fusion.2 = bf16[512,512]{1,0:T(8,128)(2,1)S(1)} fusion(bf16[512,2048]{1,0:T(8,128)(2,1)} %all-gather.7.cloned.1.call-done, bf16[2048,512]{1,0:T(8,128)(2,1)} %all-gather.9.cloned.1.call-done), kind=kOutput, calls=%fused_computation.24 | convolution fusion | flops 1074003968 | bytes 4718592 | tf_op jit(solution)/shard_map/dot_general | solution.py:62
  90.7 2.5 collective-permute-start
  93.3 1.2 collective-permute-done
  96.2 1.9 fusion.4
  98.1 1.6 copy.31
  100.9 2.3 slice.367
  103.2 2.1 slice.305
  105.3 2.1 slice.304
  107.5 19.5 %slice.303 = f32[256,512]{0,1:T(8,128)S(1)} slice(f32[512,512]{0,1:T(8,128)S(1)} %bitcast.49), slice={[1:512:2], [0:512:1]} | slice | bytes 1048576 | tf_op jit(solution)/shard_map/slice | solution.py:97
  127.0 19.4 %slice.302 = f32[255,512]{0,1:T(8,128)S(1)} slice(f32[512,512]{0,1:T(8,128)S(1)} %bitcast.50), slice={[2:512:2], [0:512:1]} | slice | bytes 1044480 | tf_op jit(solution)/shard_map/slice | solution.py:97
  146.4 19.5 %slice.307 = f32[256,512]{0,1:T(8,128)S(1)} slice(f32[512,512]{0,1:T(8,128)S(1)} %bitcast.51), slice={[0:511:2], [0:512:1]} | slice | bytes 1048576 | tf_op jit(solution)/shard_map/slice | solution.py:97
  167.3 1.3 multiply_add_fusion
  177.9 2.9 pad.144
  180.8 2.7 pad.126
  183.6 2.7 pad.127
  187.0 27.3 %all-gather.1 = f32[8,1,512]{2,1,0:T(1,128)S(1)} all-gather(f32[1,1,512]{2,1,0:T(1,128)S(1)} %add_bitcast_fusion), channel_id=1, replica_groups=mesh['sp'=8,'tp'=4] {'sp'}, dimensions={0}, use_global_device_ids=true | all-gather | bytes 18432 | tf_op jit(solution)/shard_map/all_gather | solution.py:18
  214.3 2.8 pad.145
  217.8 26.1 %all-gather = f32[8,1,512]{2,1,0:T(1,128)S(1)} all-gather(f32[1,1,512]{2,1,0:T(1,128)S(1)} %add_bitcast_fusion.1), channel_id=1, replica_groups=mesh['sp'=8,'tp'=4] {'sp'}, dimensions={0}, use_global_device_ids=true | all-gather | bytes 18432 | tf_op jit(solution)/shard_map/all_gather | solution.py:18
  244.4 7.9 %convolution_convert_fusion = bf16[512,2048]{1,0:T(8,128)(2,1)} fusion(bf16[512,2048]{1,0:T(8,128)(2,1)} %all-gather.13.cloned.1.call-done, bf16[512,2048]{1,0:T(8,128)(2,1)} %all-gather.7.cloned.1.call-done, bf16[2048,512]{1,0:T(8,128)(2,1)} %all-gather.11.cloned.1.call-done, f32[512,512]{1,0:T(8,128)S(1)} %copy-done.8, f32[512,512]{1,0:T(8,128)} %pad.145, ...), kind=kOutput, calls=%fused_computation.3 | convolution fusion | flops 2152726528 | bytes 12584960 | tf_op jit(solution)/shard_map/dot_general | solution.py:105
  252.3 28.5 %reduce-scatter.2.cloned.1.call-done = bf16[128,2048]{1,0:T(8,128)(2,1)} async-done(((bf16[512,2048]{1,0:T(8,128)(2,1)}), bf16[128,2048]{1,0:T(8,128)(2,1)}) %reduce-scatter.2.cloned.1.call-update) | async-done | bytes 524304 | tf_op jit(solution)/shard_map/reduce_scatter | solution.py:104
  (202 shorter events, 18.0 us)
Async XLA Ops:
  6.5 88.5 %copy-start = (bf16[2,256,256]{2,1,0:T(8,128)(2,1)S(1)}, bf16[2,256,256]{2,1,0:T(8,128)(2,1)}, u32[]{:S(2)}) copy-start(bf16[2,256,256]{2,1,0:T(8,128)(2,1)} %param.17) | copy-start | bytes 786436
  6.5 6.1 %copy-start.9 = (bf16[4,512]{1,0:T(4,128)(2,1)S(1)}, bf16[4,512]{1,0:T(4,128)(2,1)}, u32[]{:S(2)}) copy-start(bf16[4,512]{1,0:T(4,128)(2,1)} %param.16) | copy-start | bytes 12292
  6.5 29.5 %all-gather.7.cloned.1.call-start = ((), (), s32[]{:S(2)}) async-start(), calls=%async_computation.1 | async-start | bytes 2621440 | tf_op jit(solution)/shard_map/all_gather | solution.py:61
  10.6 76.7 %all-gather.9.cloned.1.call-start = ((), (), s32[]{:S(2)}) async-start(), calls=%async_computation.2 | async-start | bytes 2359296 | tf_op jit(solution)/shard_map/all_gather | solution.py:57
  11.3 233.0 %all-gather.11.cloned.1.call-start = ((), (), s32[]{:S(2)}) async-start(), calls=%async_computation.3 | async-start | bytes 2359296 | tf_op jit(solution)/shard_map/all_gather | solution.py:58
  12.1 232.3 %all-gather.13.cloned.1.call-start = ((), (), s32[]{:S(2)}) async-start(), calls=%async_computation.4 | async-start | bytes 2359296 | tf_op jit(solution)/shard_map/all_gather | solution.py:103
  12.6 268.2 %reduce-scatter.2.cloned.1.call-start = ((), (), s32[]{:S(2)}) async-start(), calls=%async_computation.5 | async-start | bytes 2621440 | tf_op jit(solution)/shard_map/reduce_scatter | solution.py:104
  12.7 80.5 %copy-start.10 = (f32[512]{0:T(512)S(1)}, f32[512]{0:T(512)}, u32[]{:S(2)}) copy-start(f32[512]{0:T(512)} %param.19) | copy-start | bytes 6148
  12.7 82.3 %copy-start.12 = (f32[2,512]{1,0:T(2,128)S(1)}, f32[2,512]{1,0:T(2,128)}, u32[]{:S(2)}) copy-start(f32[2,512]{1,0:T(2,128)} %param.20) | copy-start | bytes 12292
  90.7 3.8 %collective-permute-start = (bf16[3,512]{1,0:T(4,128)(2,1)S(1)}, bf16[3,512]{1,0:T(4,128)(2,1)S(1)}, u32[]{:S(2)}, u32[]{:S(2)}) collective-permute-start(bf16[3,512]{1,0:T(4,128)(2,1)S(1)} %slice.388), channel_id=1, source_target_pairs={{0,4},{4,8},{8,12},{12,16},{16,20},{20,24},{24,28},{1,5},{5,9},{9,... | collective-permute-start | bytes 9224 | tf_op jit(solution)/shard_map/ppermute | solution.py:13
  95.0 0.8 copy-start.2
  95.1 1.1 copy-start.11
  100.9 26.1 %copy-start.1 = (f32[512,512]{1,0:T(8,128)}, f32[512,512]{1,0:T(8,128)S(1)}, u32[]{:S(2)}) copy-start(f32[512,512]{1,0:T(8,128)S(1)} %convert_multiply_fusion.5) | copy-start | bytes 3145732
  165.9 1.3 copy-start.3
  165.9 1.4 copy-start.4
  175.5 1.1 copy-start.5
  175.5 1.2 copy-start.6
  177.8 2.9 %slice-start = ((f32[512,512]{1,0:T(8,128)}), f32[1,512]{1,0:T(1,128)S(1)}, s32[]{:S(2)}) async-start(f32[512,512]{1,0:T(8,128)} %copy-done.1), calls=%async_computation.6 | async-start | bytes 4096 | tf_op jit(solution)/shard_map/slice | solution.py:97
  177.8 2.9 %copy-start.7 = (f32[255,512]{1,0:T(8,128)S(1)}, f32[255,512]{1,0:T(8,128)}, u32[]{:S(2)}) copy-start(f32[255,512]{1,0:T(8,128)} %get-tuple-element.130) | copy-start | bytes 1566724
  180.8 36.3 %copy-start.8 = (f32[512,512]{1,0:T(8,128)S(1)}, f32[512,512]{1,0:T(8,128)}, u32[]{:S(2)}) copy-start(f32[512,512]{1,0:T(8,128)} %pad.144) | copy-start | bytes 3145732
Sparse Core Ops, SparseCore 0:
  10.7 25.2 all-gather.6
  38.1 49.0 all-gather.8
  89.4 47.6 all-gather.10
  139.0 48.8 all-gather.12
  252.4 28.3 reduce-scatter.1
where the time goes:
time: 288 us; the launch traced here: 287 us
  waiting for transfers between devices  106 us (37%)
  local copies, waits for them, and re-layouts  85.9 us (30%)
  blocking collectives  53.4 us (19%)
  between operations  14.1 us (5%)
  matrix products  13.9 us (5%)
  other arithmetic  10.9 us (4%)
    slice x61, local copies, waits for them, and re-layouts, on_device(): lax.associative_scan(combine_pair, (decay, drive), axis=0)  68.6 us
    all_gather x2, blocking collectives, carried_in(): everything = jax.tree.map(lambda part: lax.all_gather(part, axis), array)  53.4 us
    all_gather x1, waiting for transfers between devices, on_device(): lax.all_gather(proj_x, 'sp', axis=0, tiled=True)  51.2 us
    reduce_scatter x1, waiting for transfers between devices, on_device(): lax.psum_scatter(jnp.dot(mixed, out_cols, preferred_element_type=jnp.floa...  28.5 us
    all_gather x1, waiting for transfers between devices, on_device(): piece = lax.all_gather(normed, 'tp', axis=0, tiled=True)  23.3 us
    pad x32, local copies, waits for them, and re-layouts, on_device(): lax.associative_scan(combine_pair, (decay, drive), axis=0)  11.7 us
    dot_general x1, matrix products, on_device(): jnp.dot(mixed, out_cols, preferred_element_type=jnp.float32)  7.88 us
  transfers between devices with their start and end apart: 6, of which 4 were waited for; matrix products, arithmetic and copies ran while one was open for 34% of the time, Pallas kernels for 0%

commit v1 on v0

--- a/solution.py
+++ b/solution.py
@@ -5,6 +5,17 @@
 
 HEAD = 256
 CONV = 4
+
+
+def around_the_ring(x, axis, along):
+    size = lax.axis_size(axis)
+    right = [(i, (i + 1) % size) for i in range(size)]
+    parts = [x]
+    for far in range(1, size):
+        parts = [lax.ppermute(parts[0], axis, right), *parts]
+    whole = jnp.concatenate(parts, axis=along)
+    shift = (lax.axis_index(axis) + 1) * parts[-1].shape[along]
+    return jnp.roll(whole, shift, axis=along)
 
 
 def shifted(block, axis, distance):
@@ -58,7 +69,7 @@
         lax.all_gather(gate_projection, "sp", axis=0, tiled=True),
     )
     local_width = proj_x.shape[1]
-    piece = lax.all_gather(normed, "tp", axis=0, tiled=True)
+    piece = around_the_ring(normed, "tp", 0)
     branch_piece = jnp.dot(piece, full_x, preferred_element_type=jnp.float32).astype(jnp.bfloat16)
     gating_piece = jnp.dot(piece, full_gate, preferred_element_type=jnp.float32).astype(
         jnp.bfloat16

time: 288 us -> 348 us (1.21)
  local copies, waits for them, and re-layouts: 85.9 us -> 150 us
  waiting for transfers between devices: 106 us -> 72.8 us
  other arithmetic: 10.9 us -> 38.1 us
    slice x61 -> x60, local copies, waits for them, and re-layouts: 68.6 us -> 130 us  [on_device(): lax.associative_scan(combine_pair, (decay, drive), axis=0)]
    all_gather x1, waiting for transfers between devices: 51.2 us -> 16.5 us  [on_device(): lax.all_gather(proj_x, 'sp', axis=0, tiled=True)]
    ppermute x0 -> x3, waiting for transfers between devices: none -> 25 us  [around_the_ring(): parts = [lax.ppermute(parts[0], axis, right), *parts]]
    all_gather x1 -> x0, waiting for transfers between devices: 23.3 us -> none  [on_device(): piece = lax.all_gather(normed, 'tp', axis=0, tiled=True)]
    add x16, other arithmetic: 2.9 us -> 17.1 us  [combine_pair(): return (earlier[0] * later[0], later[0] * earlier[1] + later[1])]
    concatenate x15, other arithmetic: 0.28 us -> 7.94 us  [on_device(): lax.associative_scan(combine_pair, (decay, drive), axis=0)]
    unnamed x32 -> x46, local copies, waits for them, and re-layouts: 3.97 us -> 9.2 us
  transfers between devices with their start and end apart: 6 -> 8, of which waited for: 4 -> 6; matrix products, arithmetic and copies ran while one was open for 34% -> 56% of each run, Pallas kernels for 0% -> 0%
where the time goes in v1:
time: 348 us; the launch traced here: 344 us
  local copies, waits for them, and re-layouts  150 us (43%)
  waiting for transfers between devices  72.8 us (21%)
  blocking collectives  53.6 us (15%)
  other arithmetic  38.1 us (11%)
  between operations  13.8 us (4%)
  matrix products  12.5 us (4%)
    slice x60, local copies, waits for them, and re-layouts, on_device(): lax.associative_scan(combine_pair, (decay, drive), axis=0)  130 us
    all_gather x2, blocking collectives, carried_in(): everything = jax.tree.map(lambda part: lax.all_gather(part, axis), array)  53.6 us
    reduce_scatter x1, waiting for transfers between devices, on_device(): lax.psum_scatter(jnp.dot(mixed, out_cols, preferred_element_type=jnp.floa...  28.5 us
    ppermute x3, waiting for transfers between devices, around_the_ring(): parts = [lax.ppermute(parts[0], axis, right), *parts]  25 us
    add x16, other arithmetic, combine_pair(): return (earlier[0] * later[0], later[0] * earlier[1] + later[1])  17.1 us
    all_gather x1, waiting for transfers between devices, on_device(): lax.all_gather(proj_x, 'sp', axis=0, tiled=True)  16.5 us
    pad x32, local copies, waits for them, and re-layouts, on_device(): lax.associative_scan(combine_pair, (decay, drive), axis=0)  10.8 us
    unnamed x46, local copies, waits for them, and re-layouts  9.2 us
  transfers between devices with their start and end apart: 8, of which 6 were waited for; matrix products, arithmetic and copies ran while one was open for 56% of the time, Pallas kernels for 0%

profile of v1, /device:TPU:0, one launch (start us, length us, event | category | flops | bytes accessed | tf_op | source)
XLA Modules:
  0.0 344.5 jit_solution(547599991704164293)
XLA Ops:
  11.8 8.8 %collective-permute-done = bf16[128,2048]{1,0:T(8,128)(2,1)S(1)} collective-permute-done((bf16[128,2048]{1,0:T(8,128)(2,1)S(1)}, bf16[128,2048]{1,0:T(8,128)(2,1)S(1)}, u32[]{:S(2)}, u32[]{:S(2)}) %collective-permute-start) | collective-permute-done | bytes 524320 | tf_op jit(solution)/shard_map/ppermute | solution.py:15
  20.5 8.6 %collective-permute-done.1 = bf16[128,2048]{1,0:T(8,128)(2,1)S(1)} collective-permute-done((bf16[128,2048]{1,0:T(8,128)(2,1)S(1)}, bf16[128,2048]{1,0:T(8,128)(2,1)S(1)}, u32[]{:S(2)}, u32[]{:S(2)}) %collective-permute-start.1) | collective-permute-done | bytes 524320 | tf_op jit(solution)/shard_map/ppermute | solution.py:15
  30.1 7.7 %collective-permute-done.2 = bf16[128,2048]{1,0:T(8,128)(2,1)S(1)} collective-permute-done((bf16[128,2048]{1,0:T(8,128)(2,1)S(1)}, bf16[128,2048]{1,0:T(8,128)(2,1)S(1)}, u32[]{:S(2)}, u32[]{:S(2)}) %collective-permute-start.2) | collective-permute-done | bytes 524320 | tf_op jit(solution)/shard_map/ppermute | solution.py:15
  44.8 16.5 %all-gather.6.cloned.1.call-done = bf16[2048,512]{1,0:T(8,128)(2,1)} async-done(((bf16[256,512]{1,0:T(8,128)(2,1)}), bf16[2048,512]{1,0:T(8,128)(2,1)}) %all-gather.6.cloned.1.call-update) | async-done | bytes 2097168 | tf_op jit(solution)/shard_map/all_gather | solution.py:68
  61.3 3.5 %fusion.15 = bf16[512,512]{1,0:T(8,128)(2,1)S(1)} fusion(bf16[2048,512]{1,0:T(8,128)(2,1)} %all-gather.6.cloned.1.call-done, bf16[1024,2048]{1,0:T(8,128)(2,1)} %constant_dynamic-update-slice_fusion, s32[]{:T(128)S(6)} %select_n.40), kind=kOutput, calls=%fused_computation.27 | convolution fusion | flops 1074003968 | bytes 4718596 | tf_op jit(solution)/shard_map/dot_general | solution.py:73
  64.8 2.6 collective-permute-start.3
  72.4 2.2 slice.304
  74.7 2.1 slice.305
  76.7 19.4 %slice.303 = f32[256,512]{0,1:T(8,128)S(1)} slice(f32[512,512]{0,1:T(8,128)S(1)} %bitcast.47), slice={[1:512:2], [0:512:1]} | slice | bytes 1048576 | tf_op jit(solution)/shard_map/slice | solution.py:108
  96.2 19.5 %slice.307 = f32[256,512]{0,1:T(8,128)S(1)} slice(f32[512,512]{0,1:T(8,128)S(1)} %bitcast.48), slice={[0:511:2], [0:512:1]} | slice | bytes 1048576 | tf_op jit(solution)/shard_map/slice | solution.py:108
  117.7 1.7 multiply_add_fusion
  124.9 2.1 multiply_add_fusion.1
  133.3 1.8 multiply_add_fusion.2
  195.2 2.1 slice.367
  197.3 19.9 %slice.302 = f32[255,512]{0,1:T(8,128)} slice(f32[512,512]{0,1:T(8,128)S(1)} %bitcast.49), slice={[2:512:2], [0:512:1]} | slice | bytes 1044480 | tf_op jit(solution)/shard_map/slice | solution.py:108
  230.8 2.0 copy.35
  232.9 2.5 fusion.43
  236.4 2.1 pad.127
  239.6 2.8 pad.126
  243.1 27.5 %all-gather.1 = f32[8,1,512]{2,1,0:T(1,128)S(1)} all-gather(f32[1,1,512]{2,1,0:T(1,128)S(1)} %add_bitcast_fusion), channel_id=1, replica_groups=mesh['sp'=8,'tp'=4] {'sp'}, dimensions={0}, use_global_device_ids=true | all-gather | bytes 18432 | tf_op jit(solution)/shard_map/all_gather | solution.py:29
  270.6 2.7 pad.145
  275.3 26.1 %all-gather = f32[8,1,512]{2,1,0:T(1,128)S(1)} all-gather(f32[1,1,512]{2,1,0:T(1,128)S(1)} %add_bitcast_fusion.1), channel_id=1, replica_groups=mesh['sp'=8,'tp'=4] {'sp'}, dimensions={0}, use_global_device_ids=true | all-gather | bytes 18432 | tf_op jit(solution)/shard_map/all_gather | solution.py:29
  301.9 7.5 %convolution_convert_fusion = bf16[512,2048]{1,0:T(8,128)(2,1)} fusion(bf16[512,2048]{1,0:T(8,128)(2,1)} %all-gather.10.cloned.1.call-done, bf16[2048,512]{1,0:T(8,128)(2,1)} %all-gather.8.cloned.1.call-done, bf16[1024,2048]{1,0:T(8,128)(2,1)} %constant_dynamic-update-slice_fusion, s32[]{:T(128)S(6)} %select_n.40, f32[512,512]{1,0:T(8,128)S(1)} %pad.144, ...), kind=kOutput, calls=%fused_computation.3 | convolution fusion | flops 2152726528 | bytes 12584964 | tf_op jit(solution)/shard_map/dot_general | solution.py:116
  309.4 28.5 %reduce-scatter.2.cloned.1.call-done = bf16[128,2048]{1,0:T(8,128)(2,1)} async-done(((bf16[512,2048]{1,0:T(8,128)(2,1)}), bf16[128,2048]{1,0:T(8,128)(2,1)}) %reduce-scatter.2.cloned.1.call-update) | async-done | bytes 524304 | tf_op jit(solution)/shard_map/reduce_scatter | solution.py:115
  (220 shorter events, 110.8 us)
Async XLA Ops:
  6.5 62.7 %copy-start = (bf16[2,256,256]{2,1,0:T(8,128)(2,1)S(1)}, bf16[2,256,256]{2,1,0:T(8,128)(2,1)}, u32[]{:S(2)}) copy-start(bf16[2,256,256]{2,1,0:T(8,128)(2,1)} %param.17) | copy-start | bytes 786436
  6.5 33.8 %copy-start.1 = (bf16[128,2048]{1,0:T(8,128)(2,1)S(1)}, bf16[128,2048]{1,0:T(8,128)(2,1)}, u32[]{:S(2)}) copy-start(bf16[128,2048]{1,0:T(8,128)(2,1)} %param.12) | copy-start | bytes 1572868
  6.5 54.8 %all-gather.6.cloned.1.call-start = ((), (), s32[]{:S(2)}) async-start(), calls=%async_computation.1 | async-start | bytes 2359296 | tf_op jit(solution)/shard_map/all_gather | solution.py:68
  7.3 294.6 %all-gather.10.cloned.1.call-start = ((), (), s32[]{:S(2)}) async-start(), calls=%async_computation.3 | async-start | bytes 2359296 | tf_op jit(solution)/shard_map/all_gather | solution.py:114
  8.0 293.9 %all-gather.8.cloned.1.call-start = ((), (), s32[]{:S(2)}) async-start(), calls=%async_computation.2 | async-start | bytes 2359296 | tf_op jit(solution)/shard_map/all_gather | solution.py:69
  11.2 9.3 %collective-permute-start = (bf16[128,2048]{1,0:T(8,128)(2,1)S(1)}, bf16[128,2048]{1,0:T(8,128)(2,1)S(1)}, u32[]{:S(2)}, u32[]{:S(2)}) collective-permute-start(bf16[128,2048]{1,0:T(8,128)(2,1)S(1)} %fusion.23), channel_id=1, source_target_pairs={{0,1},{1,2},{2,3},{3,0},{4,5},{5,6},{6,7},{7,4},{8,9},{9,10},{10,1... | collective-permute-start | bytes 1572872 | tf_op jit(solution)/shard_map/ppermute | solution.py:15
  20.5 8.6 %collective-permute-start.1 = (bf16[128,2048]{1,0:T(8,128)(2,1)S(1)}, bf16[128,2048]{1,0:T(8,128)(2,1)S(1)}, u32[]{:S(2)}, u32[]{:S(2)}) collective-permute-start(bf16[128,2048]{1,0:T(8,128)(2,1)S(1)} %collective-permute-done), channel_id=1, source_target_pairs={{0,1},{1,2},{2,3},{3,0},{4,5},{5,6},{6,7},{7,4},{8,9},{9,10},{10,1... | collective-permute-start | bytes 1572872 | tf_op jit(solution)/shard_map/ppermute | solution.py:15
  29.2 8.6 %collective-permute-start.2 = (bf16[128,2048]{1,0:T(8,128)(2,1)S(1)}, bf16[128,2048]{1,0:T(8,128)(2,1)S(1)}, u32[]{:S(2)}, u32[]{:S(2)}) collective-permute-start(bf16[128,2048]{1,0:T(8,128)(2,1)S(1)} %collective-permute-done.1), channel_id=1, source_target_pairs={{0,1},{1,2},{2,3},{3,0},{4,5},{5,6},{6,7},{7,4},{8,9},{9,10},{10,1... | collective-permute-start | bytes 1572872 | tf_op jit(solution)/shard_map/ppermute | solution.py:15
  29.2 308.8 %reduce-scatter.2.cloned.1.call-start = ((), (), s32[]{:S(2)}) async-start(), calls=%async_computation.4 | async-start | bytes 2621440 | tf_op jit(solution)/shard_map/reduce_scatter | solution.py:115
  43.8 23.6 %copy-start.14 = (f32[512]{0:T(512)S(1)}, f32[512]{0:T(512)}, u32[]{:S(2)}) copy-start(f32[512]{0:T(512)} %param.19) | copy-start | bytes 6148
  44.8 24.4 %copy-start.16 = (f32[2,512]{1,0:T(2,128)S(1)}, f32[2,512]{1,0:T(2,128)}, u32[]{:S(2)}) copy-start(f32[2,512]{1,0:T(2,128)} %param.20) | copy-start | bytes 12292
  64.8 5.1 %copy-start.15 = (bf16[2,256,256]{2,1,0:T(8,128)(2,1)S(1)}, bf16[2,256,256]{2,1,0:T(8,128)(2,1)}, u32[]{:S(2)}) copy-start(bf16[2,256,256]{2,1,0:T(8,128)(2,1)} %param.18) | copy-start | bytes 786436
  64.8 3.9 %collective-permute-start.3 = (bf16[3,512]{1,0:T(4,128)(2,1)S(1)}, bf16[3,512]{1,0:T(4,128)(2,1)S(1)}, u32[]{:S(2)}, u32[]{:S(2)}) collective-permute-start(bf16[3,512]{1,0:T(4,128)(2,1)S(1)} %slice.388), channel_id=1, source_target_pairs={{0,4},{4,8},{8,12},{12,16},{16,20},{20,24},{24,28},{1,5},{5,9},{9,... | collective-permute-start | bytes 9224 | tf_op jit(solution)/shard_map/ppermute | solution.py:24
  69.9 127.5 %copy-start.2 = (f32[512,2,256]{0,2,1:T(8,128)}, f32[512,2,256]{0,2,1:T(8,128)S(1)}, u32[]{:S(2)}) copy-start(f32[512,2,256]{0,2,1:T(8,128)S(1)} %get-tuple-element.172) | copy-start | bytes 3145732
  194.7 32.8 %copy-start.7 = (f32[63,512]{1,0:T(8,128)S(1)}, f32[63,512]{1,0:T(8,128)}, u32[]{:S(2)}) copy-start(f32[63,512]{1,0:T(8,128)} %slice.363) | copy-start | bytes 387076
  195.2 30.8 %copy-start.8 = (f32[31,512]{1,0:T(8,128)S(1)}, f32[31,512]{1,0:T(8,128)}, u32[]{:S(2)}) copy-start(f32[31,512]{1,0:T(8,128)} %slice.320) | copy-start | bytes 190468
  195.2 30.8 %copy-start.9 = (f32[31,512]{1,0:T(8,128)S(1)}, f32[31,512]{1,0:T(8,128)}, u32[]{:S(2)}) copy-start(f32[31,512]{1,0:T(8,128)} %slice.361) | copy-start | bytes 190468
  222.3 5.4 %copy-start.13 = (f32[1,512]{1,0:T(1,128)S(1)}, f32[1,512]{1,0:T(1,128)}, u32[]{:S(2)}) copy-start(f32[1,512]{1,0:T(1,128)} %slice.424) | copy-start | bytes 6148
  223.7 5.6 %copy-start.5 = (f32[127,512]{1,0:T(8,128)S(1)}, f32[127,512]{1,0:T(8,128)}, u32[]{:S(2)}) copy-start(f32[127,512]{1,0:T(8,128)} %slice.308) | copy-start | bytes 780292
  223.7 5.6 %copy-start.6 = (f32[127,512]{1,0:T(8,128)S(1)}, f32[127,512]{1,0:T(8,128)}, u32[]{:S(2)}) copy-start(f32[127,512]{1,0:T(8,128)} %slice.365) | copy-start | bytes 780292
  226.7 2.7 copy-start.12
  227.6 2.0 copy-start.11
  236.3 38.1 %copy-start.4 = (f32[255,512]{1,0:T(8,128)S(1)}, f32[255,512]{1,0:T(8,128)}, u32[]{:S(2)}) copy-start(f32[255,512]{1,0:T(8,128)} %get-tuple-element.131) | copy-start | bytes 1566724
  236.4 65.1 %copy-start.10 = (f32[512]{0:T(512)S(1)}, f32[512]{0:T(512)}, u32[]{:S(2)}) copy-start(f32[512]{0:T(512)} %custom-call) | copy-start | bytes 6148
  (1 other events, 1.6 us)
Sparse Core Ops, SparseCore 0:
  9.5 51.7 all-gather.5
  63.3 48.8 all-gather.9
  114.4 47.3 all-gather.7
  309.5 28.3 reduce-scatter.1
